TPU v7x, 32 devices: a whole 2x2x4 slice. The times are simulated.
32 devices in a mesh: sp: 8 (over z, y), tp: 4 (over x, core).
Axes of the slice: x: 2, y: 2, z: 4, core: 2. Of those that a mesh axis runs over, the one named last changes fastest.
Arguments:
- tokens: bfloat16 [8192, 4096], P('sp', 'tp'), may hold values from -16 to 16
- norm_gain: float32 [4096], replicated, may hold values from 0.1 to 1.9
- w_pool_in: bfloat16 [4096, 2048], P('sp', 'tp'), may hold values from -0.09375 to 0.09375
- w_query: bfloat16 [4096, 2048], P('sp', 'tp'), may hold values from -0.09375 to 0.09375
- w_key: bfloat16 [4096, 256], P('sp', 'tp'), may hold values from -0.09375 to 0.09375
- w_value: bfloat16 [4096, 256], P('sp', 'tp'), may hold values from -0.09375 to 0.09375
- pool_map: bfloat16 [4, 512, 512], P('tp'), may hold values from -0.25 to 0.25
- pool_scale: float32 [2048], P('tp'), may hold values from 0.3 to 3
- q_gain: float32 [64], replicated, may hold values from 0.1 to 1.9
- k_gain: float32 [64], replicated, may hold values from 0.1 to 1.9
- sinks: float32 [32], P('tp'), may hold values from 0 to 4
- w_out: bfloat16 [4096, 4096], P('tp', 'sp'), may hold values from -0.09375 to 0.09375
Outputs:
- layer_out: bfloat16 [8192, 4096], P(('sp', 'tp'))
All inputs are finite; a program needn't handle non-finite values.
Results may differ from a plain program's by a relative error of at most 0.012.
Values may be sent and summed in bfloat16 or wider, within the bound.
A program may use at most 128 MiB of HBM per device.

v0:
```python
import jax
import jax.numpy as jnp
from jax import lax
from jax.sharding import PartitionSpec as P

HEAD_DIM = 64
GROUP = 8
WINDOW = 128
GROUP_WIDTH = 512
Q_HEADS = 32
epsilon = 1e-06


def passed_along(value, axis, steps):
    count = lax.axis_size(axis)
    first, last = (max(0, -steps), min(count, count - steps))
    return lax.ppermute(value, axis, [(source, source + steps) for source in range(first, last)])


def rms_scale(values):
    return values * lax.rsqrt(jnp.mean(values * values, axis=-1, keepdims=True) + epsilon)


def local(
    tokens,
    norm_gain,
    w_pool_in,
    w_query,
    w_key,
    w_value,
    pool_map,
    pool_scale,
    q_gain,
    k_gain,
    sinks,
    w_out,
):
    tok_rows = tokens.shape[0]
    local_groups = w_key.shape[1] // HEAD_DIM
    seq_index = lax.axis_index("sp")
    group_first = lax.axis_index("tp") * local_groups
    gathered = lax.all_gather(tokens, "tp", axis=1, tiled=True)
    widened = gathered.astype(jnp.float32)
    normed = (rms_scale(widened) * norm_gain).astype(jnp.bfloat16)
    ext_rows = normed.shape[0]
    pieces = (
        lax.all_gather(w_pool_in, "sp", axis=0, tiled=True),
        lax.all_gather(w_query, "sp", axis=0, tiled=True),
        lax.all_gather(w_key, "sp", axis=0, tiled=True),
        lax.all_gather(w_value, "sp", axis=0, tiled=True),
    )
    pool_sum, query_sum, key_sum, value_sum = tuple(
        (
            jnp.dot(normed, weight_piece, preferred_element_type=jnp.float32)
            for weight_piece in pieces
        )
    )
    pool_in = pool_sum.astype(jnp.bfloat16)
    query_rows = lax.optimization_barrier(query_sum.astype(jnp.bfloat16))
    key_rows = lax.optimization_barrier(key_sum.astype(jnp.bfloat16))
    value_rows = value_sum.astype(jnp.bfloat16).reshape(ext_rows, local_groups, HEAD_DIM)
    query_float = query_rows.astype(jnp.float32).reshape(ext_rows, local_groups * GROUP, HEAD_DIM)
    query_normed = (
        (rms_scale(query_float) * q_gain)
        .astype(jnp.bfloat16)
        .reshape(ext_rows, local_groups, GROUP, HEAD_DIM)
    )
    key_float = key_rows.astype(jnp.float32).reshape(ext_rows, local_groups, HEAD_DIM)
    key_normed = (rms_scale(key_float) * k_gain).astype(jnp.bfloat16)
    key_width = local_groups * HEAD_DIM
    pair_tail = jnp.concatenate(
        [
            key_normed[tok_rows - WINDOW :].reshape(WINDOW, key_width),
            value_rows[tok_rows - WINDOW :].reshape(WINDOW, key_width),
        ],
        axis=1,
    )
    earlier_pairs, earlier_pool = passed_along((pair_tail, pool_in[tok_rows - 15 :]), "sp", 1)
    key_span = jnp.concatenate(
        [earlier_pairs[:, :key_width].reshape(WINDOW, local_groups, HEAD_DIM), key_normed], axis=0
    )
    value_span = jnp.concatenate(
        [earlier_pairs[:, key_width:].reshape(WINDOW, local_groups, HEAD_DIM), value_rows], axis=0
    )
    pool_span = jnp.concatenate([earlier_pool, pool_in], axis=0)
    positions = seq_index * tok_rows + jnp.arange(tok_rows, dtype=jnp.int32)
    group_ids = group_first + jnp.arange(local_groups, dtype=jnp.int32)
    spans = jnp.exp2((group_ids + 1).astype(jnp.float32))
    pool_float = pool_span.astype(jnp.float32).reshape(tok_rows + 15, local_groups, GROUP_WIDTH)
    sum_two = pool_float[1:] + pool_float[:-1]
    sum_four = sum_two[2:] + sum_two[:-2]
    sum_eight = sum_four[4:] + sum_four[:-4]
    sum_sixteen = sum_eight[8:] + sum_eight[:-8]
    span_pick = spans[None, :, None]
    running = jnp.where(
        span_pick < 3.0,
        sum_two[14 : 14 + tok_rows],
        jnp.where(
            span_pick < 6.0,
            sum_four[12 : 12 + tok_rows],
            jnp.where(span_pick < 12.0, sum_eight[8 : 8 + tok_rows], sum_sixteen),
        ),
    )
    counts = jnp.minimum(positions.astype(jnp.float32)[:, None] + 1.0, spans[None, :])
    pool_diff = (running / counts[:, :, None] - pool_float[15:]).astype(jnp.bfloat16)
    mapped = jnp.einsum("tlc,lcd->tld", pool_diff, pool_map, preferred_element_type=jnp.float32)
    pool_branch = rms_scale(mapped * pool_scale.reshape(local_groups, GROUP_WIDTH))
    blocks = tok_rows // WINDOW
    query_blocks = query_normed.reshape(blocks, WINDOW, local_groups, GROUP, HEAD_DIM)
    key_pairs = jnp.concatenate(
        [
            key_span[:tok_rows].reshape(blocks, WINDOW, local_groups, HEAD_DIM),
            key_span[WINDOW:].reshape(blocks, WINDOW, local_groups, HEAD_DIM),
        ],
        axis=1,
    )
    value_pairs = jnp.concatenate(
        [
            value_span[:tok_rows].reshape(blocks, WINDOW, local_groups, HEAD_DIM),
            value_span[WINDOW:].reshape(blocks, WINDOW, local_groups, HEAD_DIM),
        ],
        axis=1,
    )
    scores = jnp.einsum(
        "nqlgd,nkld->nlgqk", query_blocks, key_pairs, preferred_element_type=jnp.float32
    ) * HEAD_DIM ** (-0.5)
    query_pos = jnp.arange(WINDOW, dtype=jnp.int32)[:, None] + WINDOW
    key_pos = jnp.arange(2 * WINDOW, dtype=jnp.int32)[None, :]
    distance = query_pos - key_pos
    in_band = (distance >= 0) & (distance < WINDOW)
    key_global = (
        seq_index * tok_rows
        + jnp.arange(blocks, dtype=jnp.int32)[:, None] * WINDOW
        - WINDOW
        + jnp.arange(2 * WINDOW, dtype=jnp.int32)[None, :]
    )
    allowed = in_band[None] & (key_global >= 0)[:, None, :]
    head_ids = group_ids[:, None] * GROUP + jnp.arange(GROUP, dtype=jnp.int32)[None, :] + 1
    slopes = jnp.exp2(-8.0 * head_ids.astype(jnp.float32) / Q_HEADS)
    logits = (
        scores - slopes[None, :, :, None, None] * distance.astype(jnp.float32)[None, None, None]
    )
    exp_scores = jnp.exp(jnp.where(allowed[:, None, None], logits, -jnp.inf))
    sink_logits = sinks.reshape(local_groups, GROUP)
    denominator = jnp.sum(exp_scores, axis=-1) + jnp.exp(sink_logits)[None, :, :, None]
    weights_bf = (exp_scores / denominator[..., None]).astype(jnp.bfloat16)
    attended = jnp.einsum(
        "nlgqk,nkld->nqlgd", weights_bf, value_pairs, preferred_element_type=jnp.float32
    )
    attn_branch = rms_scale(attended.reshape(tok_rows, local_groups, GROUP_WIDTH))
    mixed_rows = (
        jnp.stack([pool_branch, attn_branch], axis=2)
        .reshape(tok_rows, 2 * local_groups * GROUP_WIDTH)
        .astype(jnp.bfloat16)
    )
    out_columns = lax.all_gather(w_out, "sp", axis=1, tiled=True)
    return lax.psum_scatter(
        jnp.dot(mixed_rows, out_columns, preferred_element_type=jnp.float32).astype(jnp.bfloat16),
        "tp",
        scatter_dimension=0,
        tiled=True,
    )


def solution(mesh):
    in_specs = (
        P("sp", "tp"),
        P(),
        P("sp", "tp"),
        P("sp", "tp"),
        P("sp", "tp"),
        P("sp", "tp"),
        P("tp", None, None),
        P("tp"),
        P(),
        P(),
        P("tp"),
        P("tp", "sp"),
    )
    out_specs = P(("sp", "tp"), None)
    return jax.shard_map(local, mesh=mesh, in_specs=in_specs, out_specs=out_specs, check_vma=False)
```

profile of v0, /device:TPU:0, one launch (start us, length us, event | category | flops | bytes accessed | tf_op | source)
XLA Modules:
  0.0 435.6 jit_solution(6995739875760048080)
XLA Ops:
  6.5 0.0 copy-start
  6.5 0.0 all-gather.5.cloned.1.call-start
  6.5 0.7 all-gather.5.cloned.1.call-update
  7.3 0.0 all-gather.7.cloned.1.call-start
  7.3 0.7 all-gather.7.cloned.1.call-update
  8.0 0.0 all-gather.9.cloned.1.call-start
  8.1 0.7 all-gather.9.cloned.1.call-update
  8.8 0.0 all-gather.11.cloned.1.call-start
  8.8 0.5 all-gather.11.cloned.1.call-update
  9.3 0.0 reduce-scatter.2.cloned.1.call-start
  9.6 33.1 %all_gather.20 = bf16[4096,64]{0,1:T(8,128)(2,1)S(1)} all-gather(bf16[512,64]{0,1:T(8,128)(2,1)S(1)} %copy-done.7), channel_id=1, replica_groups=mesh['sp'=8,'tp'=4] {'sp'}, dimensions={0}, use_global_device_ids=true | all-gather | bytes 589824 | tf_op jit(solution)/shard_map/all_gather | solution.py:49
  42.7 0.0 copy-done.8
  42.7 31.2 %all_gather.21 = bf16[4096,64]{0,1:T(8,128)(2,1)S(1)} all-gather(bf16[512,64]{0,1:T(8,128)(2,1)S(1)} %copy-done.8), channel_id=1, replica_groups=mesh['sp'=8,'tp'=4] {'sp'}, dimensions={0}, use_global_device_ids=true | all-gather | bytes 589824 | tf_op jit(solution)/shard_map/all_gather | solution.py:50
  73.9 0.1 add_compare_fusion
  74.0 1.1 broadcast_multiply_fusion
  75.1 0.3 broadcast_and_fusion
  75.4 0.0 copy-start.9
  75.4 0.0 all-gather.5.cloned.1.call-done
  75.5 5.1 %fusion = f32[1024]{0:T(1024)S(1)} fusion(bf16[1024,4096]{1,0:T(8,128)(2,1)} %all-gather.5.cloned.1.call-done), kind=kLoop, calls=%fused_computation.2 | loop fusion | flops 12581888 | bytes 8392704 | tf_op jit(solution)/shard_map/reduce_sum | solution.py:21
  80.6 10.5 %fusion.2 = bf16[1024,4096]{1,0:T(8,128)(2,1)} fusion(bf16[1024,4096]{1,0:T(8,128)(2,1)} %all-gather.5.cloned.1.call-done, f32[4096]{0:T(1024)S(1)} %copy-done.9, f32[1024]{0:T(1024)S(1)} %add_rsqrt_fusion.2), kind=kLoop, calls=%fused_computation.4 | loop fusion | flops 16777216 | bytes 16797696 | tf_op jit(solution)/shard_map/convert_element_type | solution.py:44
  91.0 53.8 %all-gather.7.cloned.1.call-done = bf16[4096,512]{1,0:T(8,128)(2,1)} async-done(((bf16[512,512]{1,0:T(8,128)(2,1)}), bf16[4096,512]{1,0:T(8,128)(2,1)}) %all-gather.7.cloned.1.call-update) | async-done | bytes 4194320 | tf_op jit(solution)/shard_map/all_gather | solution.py:47
  144.9 9.2 %convolution_convert_fusion.2 = bf16[1024,512]{1,0:T(8,128)(2,1)S(1)} fusion(bf16[1024,4096]{1,0:T(8,128)(2,1)} %fusion.2, bf16[4096,512]{1,0:T(8,128)(2,1)} %all-gather.7.cloned.1.call-done), kind=kOutput, calls=%fused_computation.32 | convolution fusion | flops 4295491584 | bytes 13631488 | tf_op jit(solution)/shard_map/dot_general | solution.py:54
  154.1 0.0 copy-start.4
  154.1 0.0 copy-start.10
  154.1 2.8 collective-permute-start
  156.9 2.7 convolution_convert_fusion.4
  159.7 0.1 fusion.24
  159.8 2.7 convolution_convert_fusion.3
  162.4 4.0 collective-permute-start.1
  166.4 53.0 %all-gather.9.cloned.1.call-done = bf16[4096,512]{1,0:T(8,128)(2,1)} async-done(((bf16[512,512]{1,0:T(8,128)(2,1)}), bf16[4096,512]{1,0:T(8,128)(2,1)}) %all-gather.9.cloned.1.call-update) | async-done | bytes 4194320 | tf_op jit(solution)/shard_map/all_gather | solution.py:48
  219.4 10.0 %convolution_convert_fusion.1 = bf16[1024,512]{1,0:T(8,128)(2,1)} fusion(bf16[1024,4096]{1,0:T(8,128)(2,1)} %fusion.2, bf16[4096,512]{1,0:T(8,128)(2,1)} %all-gather.9.cloned.1.call-done), kind=kOutput, calls=%fused_computation.31 | convolution fusion | flops 4295491584 | bytes 13631488 | tf_op jit(solution)/shard_map/dot_general | solution.py:54
  229.4 1.5 copy.24
  230.9 2.9 convert_multiply_fusion.2
  233.8 2.9 copy.25
  236.7 1.8 bitcast_reduce_fusion
  238.6 0.0 copy-start.12
  238.6 0.5 copy.37
  239.1 0.1 fusion.49
  239.2 0.1 copy-done.12
  239.3 0.3 multiply_convert_fusion.1
  239.5 0.1 fusion.50
  239.8 0.0 collective-permute-done
  239.8 0.7 copy-done.5
  240.5 0.3 maximum_convert_fusion
  240.8 0.3 slice_add_fusion.1
  241.1 0.3 slice_add_fusion
  241.4 0.0 copy-start.11
  241.4 0.3 slice_add_fusion.2
  241.7 0.4 copy-done.11
  242.1 1.4 multiply_reduce_fusion.1
  243.5 1.3 fusion.16
  244.8 0.0 collective-permute-done.1
  244.9 2.5 fusion.5
  247.4 0.1 broadcast_add_fusion
  247.5 2.4 multiply_reduce_fusion
  249.9 2.5 copy.29
  252.4 1.7 reshape.363
  254.2 0.3 multiply_convert_fusion
  254.5 0.9 copy-done.3
  255.4 0.2 pad_maximum_fusion
  255.6 89.2 %all-gather.11.cloned.1.call-done = bf16[1024,4096]{1,0:T(8,128)(2,1)} async-done(((bf16[1024,512]{1,0:T(8,128)(2,1)}), bf16[1024,4096]{1,0:T(8,128)(2,1)}) %all-gather.11.cloned.1.call-update) | async-done | bytes 8388624 | tf_op jit(solution)/shard_map/all_gather | solution.py:156
  344.8 14.5 %convolution_convert_fusion = bf16[1024,4096]{1,0:T(8,128)(2,1)} fusion(bf16[1024,1024]{0,1:T(8,128)(2,1)S(1)} %bitcast.121, bf16[1024,4096]{1,0:T(8,128)(2,1)} %all-gather.11.cloned.1.call-done), kind=kOutput, calls=%fused_computation.9 | convolution fusion | flops 8594128896 | bytes 18874368 | tf_op jit(solution)/shard_map/dot_general | solution.py:158
  359.3 0.0 reduce-scatter.2.cloned.1.call-update
  359.3 69.7 %reduce-scatter.2.cloned.1.call-done = bf16[256,4096]{1,0:T(8,128)(2,1)} async-done(((bf16[1024,4096]{1,0:T(8,128)(2,1)}), bf16[256,4096]{1,0:T(8,128)(2,1)}) %reduce-scatter.2.cloned.1.call-update) | async-done | bytes 2097168 | tf_op jit(solution)/shard_map/reduce_scatter | solution.py:157
  (43 shorter events, 0.4 us)
Async XLA Ops:
  6.5 235.2 %copy-start = (bf16[1,512,512]{2,1,0:T(8,128)(2,1)S(1)}, bf16[1,512,512]{2,1,0:T(8,128)(2,1)}, u32[]{:S(2)}) copy-start(bf16[1,512,512]{2,1,0:T(8,128)(2,1)} %param.18) | copy-start | bytes 1572868
  6.5 3.0 copy-start.7
  6.5 36.1 %copy-start.8 = (bf16[512,64]{0,1:T(8,128)(2,1)S(1)}, bf16[512,64]{0,1:T(8,128)(2,1)}, u32[]{:S(2)}) copy-start(bf16[512,64]{0,1:T(8,128)(2,1)} %param.17) | copy-start | bytes 196612
  6.5 68.9 %all-gather.5.cloned.1.call-start = ((), (), s32[]{:S(2)}) async-start(), calls=%async_computation.1 | async-start | bytes 10485760 | tf_op jit(solution)/shard_map/all_gather | solution.py:42
  7.3 66.7 %copy-start.13 = (f32[8]{0:T(128)S(1)}, f32[8]{0:T(128)}, u32[]{:S(2)}) copy-start(f32[8]{0:T(128)} %param.22) | copy-start | bytes 100
  7.3 137.6 %all-gather.7.cloned.1.call-start = ((), (), s32[]{:S(2)}) async-start(), calls=%async_computation.2 | async-start | bytes 4718592 | tf_op jit(solution)/shard_map/all_gather | solution.py:47
  8.0 211.4 %all-gather.9.cloned.1.call-start = ((), (), s32[]{:S(2)}) async-start(), calls=%async_computation.3 | async-start | bytes 4718592 | tf_op jit(solution)/shard_map/all_gather | solution.py:48
  8.8 336.1 %all-gather.11.cloned.1.call-start = ((), (), s32[]{:S(2)}) async-start(), calls=%async_computation.4 | async-start | bytes 9437184 | tf_op jit(solution)/shard_map/all_gather | solution.py:156
  9.3 419.7 %reduce-scatter.2.cloned.1.call-start = ((), (), s32[]{:S(2)}) async-start(), calls=%async_computation.5 | async-start | bytes 10485760 | tf_op jit(solution)/shard_map/reduce_scatter | solution.py:157
  75.4 5.1 %copy-start.9 = (f32[4096]{0:T(1024)S(1)}, f32[4096]{0:T(1024)}, u32[]{:S(2)}) copy-start(f32[4096]{0:T(1024)} %param.13) | copy-start | bytes 49156
  144.9 12.0 %copy-start.2 = (bf16[1024,4096]{1,0:T(8,128)(2,1)S(1)}, bf16[1024,4096]{1,0:T(8,128)(2,1)}, u32[]{:S(2)}) copy-start(bf16[1024,4096]{1,0:T(8,128)(2,1)} %fusion.2) | copy-start | bytes 25165828
  154.1 5.5 %copy-start.4 = (bf16[1024,512]{1,0:T(8,128)(2,1)}, bf16[1024,512]{1,0:T(8,128)(2,1)S(1)}, u32[]{:S(2)}) copy-start(bf16[1024,512]{1,0:T(8,128)(2,1)S(1)} %convolution_convert_fusion.2) | copy-start | bytes 3145732
  154.1 5.5 %copy-start.10 = (f32[64]{0:T(128)S(1)}, f32[64]{0:T(128)}, u32[]{:S(2)}) copy-start(f32[64]{0:T(128)} %param.21) | copy-start | bytes 772
  154.1 85.6 %collective-permute-start = (bf16[15,512]{1,0:T(8,128)(2,1)S(1)}, bf16[15,512]{1,0:T(8,128)(2,1)S(1)}, u32[]{:S(2)}, u32[]{:S(2)}) collective-permute-start(bf16[15,512]{1,0:T(8,128)(2,1)S(1)} %slice.86), channel_id=1, source_target_pairs={{0,4},{4,8},{8,12},{12,16},{16,20},{20,24},{24,28},{1,5},{5,9},{9,... | collective-permute-start | bytes 46088 | tf_op jit(solution)/shard_map/ppermute | solution.py:17
  162.4 82.3 %collective-permute-start.1 = (bf16[128,128]{0,1:T(8,128)(2,1)S(1)}, bf16[128,128]{0,1:T(8,128)(2,1)S(1)}, u32[]{:S(2)}, u32[]{:S(2)}) collective-permute-start(bf16[128,128]{0,1:T(8,128)(2,1)S(1)} %pad_maximum_fusion.3), channel_id=1, source_target_pairs={{0,4},{4,8},{8,12},{12,16},{16,20},{20,24},{24,28},{1,5},{5,9},{9,... | collective-permute-start | bytes 98312 | tf_op jit(solution)/shard_map/ppermute | solution.py:17
  238.6 0.7 copy-start.12
  239.3 1.2 copy-start.5
  241.4 0.7 copy-start.11
  243.5 1.4 copy-start.6
  254.2 1.2 copy-start.3
  359.3 69.8 %copy-start.1 = (bf16[1,512,512]{2,1,0:T(8,128)(2,1)S(1)}, bf16[1,512,512]{2,1,0:T(8,128)(2,1)}, u32[]{:S(2)}) copy-start(bf16[1,512,512]{2,1,0:T(8,128)(2,1)} %param.18) | copy-start | bytes 1572868
Sparse Core Ops, SparseCore 0:
  8.9 60.9 all-gather.4
  72.0 72.7 all-gather.6
  147.0 72.3 all-gather.8
  221.3 123.4 all-gather.10
  359.4 69.5 reduce-scatter.1
where the time goes:
time: 436 us
  waiting for transfers between devices  268 us (61%)
  blocking collectives  64.3 us (15%)
  matrix products  45.3 us (10%)
  other arithmetic  25.5 us (6%)
  between operations  13.6 us (3%)
  local copies, waits for them, and re-layouts  11.5 us (3%)
  starting transfers between devices  6.92 us (2%)
    all_gather x1, waiting for transfers between devices, local(): out_columns = lax.all_gather(w_out, 'sp', axis=1, tiled=True)  89.2 us
    reduce_scatter x1, waiting for transfers between devices, local(): lax.psum_scatter(jnp.dot(mixed_rows, out_columns, preferred_element_type=...  69.7 us
    all_gather x1, waiting for transfers between devices, local(): lax.all_gather(w_pool_in, 'sp', axis=0, tiled=True)  53.8 us
    all_gather x1, waiting for transfers between devices, local(): lax.all_gather(w_query, 'sp', axis=0, tiled=True)  53 us
    all_gather x1, blocking collectives, local(): lax.all_gather(w_key, 'sp', axis=0, tiled=True)  33.1 us
    all_gather x1, blocking collectives, local(): lax.all_gather(w_value, 'sp', axis=0, tiled=True)  31.2 us
    dot_general x4, matrix products, local(): jnp.dot(normed, weight_piece, preferred_element_type=jnp.float32)  24.5 us
    dot_general x1, matrix products, local(): jnp.dot(mixed_rows, out_columns, preferred_element_type=jnp.float32)  14.5 us
  transfers between devices with their start and end apart: 7, of which 4 were waited for; matrix products, arithmetic and copies ran while one was open for 15% of the time, Pallas kernels for 0%

commit v1 on v0

--- a/solution.py
+++ b/solution.py
@@ -9,6 +9,23 @@
 GROUP_WIDTH = 512
 Q_HEADS = 32
 epsilon = 1e-06
+
+
+def joined_along(tiles, dim):
+    lengths = list(tiles.shape[1:])
+    lengths[dim] *= tiles.shape[0]
+    return jnp.moveaxis(tiles, 0, dim).reshape(lengths)
+
+
+def gather_around(array, axis, dim):
+    devices = lax.axis_size(axis)
+    forward = [(i, (i + 1) % devices) for i in range(devices)]
+    pieces = [array]
+    while len(pieces) < devices:
+        pieces.append(lax.ppermute(pieces[-1], axis, forward))
+    here = lax.axis_index(axis)
+    pieces = jnp.stack(pieces)[(here - jnp.arange(devices)) % devices]
+    return joined_along(pieces, dim)
 
 
 def passed_along(value, axis, steps):
@@ -45,7 +62,7 @@
     ext_rows = normed.shape[0]
     pieces = (
         lax.all_gather(w_pool_in, "sp", axis=0, tiled=True),
-        lax.all_gather(w_query, "sp", axis=0, tiled=True),
+        gather_around(w_query, "sp", 0),
         lax.all_gather(w_key, "sp", axis=0, tiled=True),
         lax.all_gather(w_value, "sp", axis=0, tiled=True),
     )

time: 436 us -> 397 us (0.911)
  waiting for transfers between devices: 268 us -> 191 us
  blocking collectives: 64.3 us -> 92.3 us
  local copies, waits for them, and re-layouts: 11.5 us -> 25.1 us
  matrix products: 45.3 us -> 40.8 us
    ppermute x0 -> x7, waiting for transfers between devices: none -> 76.3 us  [gather_around(): pieces.append(lax.ppermute(pieces[-1], axis, forward))]
    all_gather x1, waiting for transfers between devices: 53.8 us -> 0.01 us  [local(): lax.all_gather(w_pool_in, 'sp', axis=0, tiled=True)]
    all_gather x1 -> x0, waiting for transfers between devices: 53 us -> none  [local(): lax.all_gather(w_query, 'sp', axis=0, tiled=True)]
    all_gather x1, waiting for transfers between devices: 89.2 us -> 44 us  [local(): out_columns = lax.all_gather(w_out, 'sp', axis=1, tiled=True)]
    all_gather x1, blocking collectives: 31.2 us -> 51.2 us  [local(): lax.all_gather(w_value, 'sp', axis=0, tiled=True)]
    all_gather x1, blocking collectives: 33.1 us -> 41.2 us  [local(): lax.all_gather(w_key, 'sp', axis=0, tiled=True)]
    unnamed x31 -> x40, local copies, waits for them, and re-layouts: 2.68 us -> 9.74 us
    gather x0 -> x1, local copies, waits for them, and re-layouts: none -> 4.94 us  [gather_around(): pieces = jnp.stack(pieces)[(here - jnp.arange(devices)) % devices]]
  transfers between devices with their start and end apart: 7 -> 13, of which waited for: 4 -> 7; matrix products, arithmetic and copies ran while one was open for 15% -> 19% of each run, Pallas kernels for 0% -> 0%
where the time goes in v1:
time: 397 us; the launch traced here: 396 us
  waiting for transfers between devices  191 us (48%)
  blocking collectives  92.3 us (23%)
  matrix products  40.8 us (10%)
  other arithmetic  26.8 us (7%)
  local copies, waits for them, and re-layouts  25.1 us (6%)
  between operations  13.7 us (3%)
  starting transfers between devices  6.19 us (2%)
    ppermute x7, waiting for transfers between devices, gather_around(): pieces.append(lax.ppermute(pieces[-1], axis, forward))  76.3 us
    reduce_scatter x1, waiting for transfers between devices, local(): lax.psum_scatter(jnp.dot(mixed_rows, out_columns, preferred_element_type=...  69.7 us
    all_gather x1, blocking collectives, local(): lax.all_gather(w_value, 'sp', axis=0, tiled=True)  51.2 us
    all_gather x1, waiting for transfers between devices, local(): out_columns = lax.all_gather(w_out, 'sp', axis=1, tiled=True)  44 us
    all_gather x1, blocking collectives, local(): lax.all_gather(w_key, 'sp', axis=0, tiled=True)  41.2 us
    dot_general x4, matrix products, local(): jnp.dot(normed, weight_piece, preferred_element_type=jnp.float32)  20 us
    dot_general x1, matrix products, local(): jnp.dot(mixed_rows, out_columns, preferred_element_type=jnp.float32)  14.5 us
    convert_element_type x1, other arithmetic, local(): normed = (rms_scale(widened) * norm_gain).astype(jnp.bfloat16)  10.4 us
  transfers between devices with their start and end apart: 13, of which 7 were waited for; matrix products, arithmetic and copies ran while one was open for 19% of the time, Pallas kernels for 0%

profile of v1, /device:TPU:0, one launch (start us, length us, event | category | flops | bytes accessed | tf_op | source)
XLA Modules:
  0.0 396.1 jit_solution(10496284695233939247)
XLA Ops:
  6.5 0.7 all-gather.4.cloned.1.call-update
  7.3 0.0 all-gather.6.cloned.1.call-start
  7.3 0.7 all-gather.6.cloned.1.call-update
  8.0 0.0 all-gather.8.cloned.1.call-start
  8.1 3.0 collective-permute-start.2
  11.1 0.0 reduce-scatter.2.cloned.1.call-start
  11.3 15.0 %collective-permute-done.2 = bf16[512,512]{1,0:T(8,128)(2,1)S(1)} collective-permute-done((bf16[512,512]{1,0:T(8,128)(2,1)}, bf16[512,512]{1,0:T(8,128)(2,1)S(1)}, u32[]{:S(2)}, u32[]{:S(2)}) %collective-permute-start.2) | collective-permute-done | bytes 524320 | tf_op jit(solution)/shard_map/ppermute | solution.py:25
  26.3 0.1 add_compare_fusion
  26.4 15.7 %collective-permute-done.3 = bf16[512,512]{1,0:T(8,128)(2,1)S(1)} collective-permute-done((bf16[512,512]{1,0:T(8,128)(2,1)S(1)}, bf16[512,512]{1,0:T(8,128)(2,1)S(1)}, u32[]{:S(2)}, u32[]{:S(2)}) %collective-permute-start.3) | collective-permute-done | bytes 524320 | tf_op jit(solution)/shard_map/ppermute | solution.py:25
  42.1 41.2 %all_gather.17 = bf16[4096,64]{0,1:T(8,128)(2,1)S(1)} all-gather(bf16[512,64]{0,1:T(8,128)(2,1)} %param.16), channel_id=1, replica_groups=mesh['sp'=8,'tp'=4] {'sp'}, dimensions={0}, use_global_device_ids=true | all-gather | bytes 589824 | tf_op jit(solution)/shard_map/all_gather | solution.py:66
  83.3 0.1 collective-permute-start.5
  83.3 0.7 copy-done.8
  84.1 51.2 %all_gather.18 = bf16[4096,64]{0,1:T(8,128)(2,1)S(1)} all-gather(bf16[512,64]{0,1:T(8,128)(2,1)S(1)} %copy-done.10), channel_id=1, replica_groups=mesh['sp'=8,'tp'=4] {'sp'}, dimensions={0}, use_global_device_ids=true | all-gather | bytes 589824 | tf_op jit(solution)/shard_map/all_gather | solution.py:67
  135.2 0.3 broadcast_and_fusion
  135.6 0.1 collective-permute-start.6
  135.7 0.7 exp.8
  136.4 0.8 bitcast_dynamic-update-slice_fusion.7
  137.3 1.1 broadcast_multiply_fusion
  138.4 20.9 %collective-permute-done.6 = bf16[512,512]{1,0:T(8,128)(2,1)} collective-permute-done((bf16[512,512]{1,0:T(8,128)(2,1)}, bf16[512,512]{1,0:T(8,128)(2,1)}, u32[]{:S(2)}, u32[]{:S(2)}) %collective-permute-start.6) | collective-permute-done | bytes 524320 | tf_op jit(solution)/shard_map/ppermute | solution.py:25
  159.3 0.8 bitcast_dynamic-update-slice_fusion.6
  160.2 0.8 bitcast_dynamic-update-slice_fusion.5
  161.0 0.8 bitcast_dynamic-update-slice_fusion.4
  161.8 17.2 %collective-permute-done.7 = bf16[512,512]{1,0:T(8,128)(2,1)S(1)} collective-permute-done((bf16[512,512]{1,0:T(8,128)(2,1)}, bf16[512,512]{1,0:T(8,128)(2,1)S(1)}, u32[]{:S(2)}, u32[]{:S(2)}) %collective-permute-start.7) | collective-permute-done | bytes 524320 | tf_op jit(solution)/shard_map/ppermute | solution.py:25
  179.1 1.9 bitcast_dynamic-update-slice_fusion.3
  181.0 1.9 bitcast_dynamic-update-slice_fusion.2
  182.8 0.8 bitcast_dynamic-update-slice_fusion.1
  183.7 7.4 %collective-permute-done.8 = bf16[512,512]{1,0:T(8,128)(2,1)S(1)} collective-permute-done((bf16[512,512]{1,0:T(8,128)(2,1)S(1)}, bf16[512,512]{1,0:T(8,128)(2,1)S(1)}, u32[]{:S(2)}, u32[]{:S(2)}) %collective-permute-start.8) | collective-permute-done | bytes 524320 | tf_op jit(solution)/shard_map/ppermute | solution.py:25
  191.1 0.8 bitcast_dynamic-update-slice_fusion
  191.9 4.9 %gather_fusion = bf16[8,512,512]{2,1,0:T(8,128)(2,1)} fusion(bf16[8,512,512]{2,1,0:T(8,128)(2,1)} %bitcast_dynamic-update-slice_fusion, s32[1024]{0:T(1024)S(1)} %pad_clamp_fusion), kind=kCustom, calls=%fused_computation | custom fusion | bytes 8388640 | tf_op jit(solution)/shard_map/gather | solution.py:27
  196.8 5.1 %fusion = f32[1024]{0:T(1024)S(1)} fusion(bf16[1024,4096]{1,0:T(8,128)(2,1)} %all-gather.4.cloned.1.call-done), kind=kLoop, calls=%fused_computation.3 | loop fusion | flops 12581888 | bytes 8392704 | tf_op jit(solution)/shard_map/reduce_sum | solution.py:38
  201.9 10.4 %fusion.2 = bf16[1024,4096]{1,0:T(8,128)(2,1)} fusion(bf16[1024,4096]{1,0:T(8,128)(2,1)} %all-gather.4.cloned.1.call-done, f32[4096]{0:T(1024)S(1)} %copy-done.11, f32[1024]{0:T(1024)S(1)} %add_rsqrt_fusion.2), kind=kLoop, calls=%fused_computation.5 | loop fusion | flops 16777216 | bytes 16797696 | tf_op jit(solution)/shard_map/convert_element_type | solution.py:61
  212.4 9.2 %convolution_convert_fusion.2 = bf16[1024,512]{1,0:T(8,128)(2,1)S(1)} fusion(bf16[1024,4096]{1,0:T(8,128)(2,1)} %fusion.2, bf16[4096,512]{1,0:T(8,128)(2,1)} %all-gather.6.cloned.1.call-done), kind=kOutput, calls=%fused_computation.33 | convolution fusion | flops 4295491584 | bytes 13631488 | tf_op jit(solution)/shard_map/dot_general | solution.py:71
  221.7 1.6 collective-permute-start
  223.3 2.7 convolution_convert_fusion.4
  226.0 0.1 fusion.24
  226.1 2.7 convolution_convert_fusion.3
  228.8 1.3 collective-permute-start.1
  230.1 5.5 %convolution_convert_fusion.1 = bf16[1024,512]{1,0:T(8,128)(2,1)} fusion(bf16[1024,4096]{1,0:T(8,128)(2,1)S(1)} %copy-done.2, bf16[4096,512]{1,0:T(8,128)(2,1)S(1)} %bitcast.140), kind=kOutput, calls=%fused_computation.32 | convolution fusion | flops 4295491584 | bytes 13631488 | tf_op jit(solution)/shard_map/dot_general | solution.py:71
  235.6 1.5 copy.24
  237.1 2.9 convert_multiply_fusion.2
  240.0 3.0 copy.25
  242.9 1.8 bitcast_reduce_fusion
  244.8 0.5 copy.37
  245.3 0.1 fusion.51
  245.4 0.3 multiply_convert_fusion.1
  245.7 0.1 fusion.52
  245.9 0.1 copy-done.5
  246.0 0.3 maximum_convert_fusion
  246.4 0.3 slice_add_fusion.1
  246.6 0.3 slice_add_fusion
  246.9 0.3 slice_add_fusion.2
  247.2 0.4 copy-done.13
  247.6 1.4 multiply_reduce_fusion.1
  249.0 1.3 fusion.16
  250.5 2.5 fusion.5
  253.0 0.1 broadcast_add_fusion
  253.0 2.4 multiply_reduce_fusion
  255.5 2.5 copy.29
  258.0 1.7 reshape.416
  259.7 0.3 multiply_convert_fusion
  260.0 1.4 pad_maximum_fusion
  261.4 44.0 %all-gather.8.cloned.1.call-done = bf16[1024,4096]{1,0:T(8,128)(2,1)} async-done(((bf16[1024,512]{1,0:T(8,128)(2,1)}), bf16[1024,4096]{1,0:T(8,128)(2,1)}) %all-gather.8.cloned.1.call-update) | async-done | bytes 8388624 | tf_op jit(solution)/shard_map/all_gather | solution.py:173
  305.4 14.5 %convolution_convert_fusion = bf16[1024,4096]{1,0:T(8,128)(2,1)} fusion(bf16[1024,1024]{0,1:T(8,128)(2,1)S(1)} %bitcast.141, bf16[1024,4096]{1,0:T(8,128)(2,1)} %all-gather.8.cloned.1.call-done), kind=kOutput, calls=%fused_computation.10 | convolution fusion | flops 8594128896 | bytes 18874368 | tf_op jit(solution)/shard_map/dot_general | solution.py:175
  319.9 69.7 %reduce-scatter.2.cloned.1.call-done = bf16[256,4096]{1,0:T(8,128)(2,1)} async-done(((bf16[1024,4096]{1,0:T(8,128)(2,1)}), bf16[256,4096]{1,0:T(8,128)(2,1)}) %reduce-scatter.2.cloned.1.call-update) | async-done | bytes 2097168 | tf_op jit(solution)/shard_map/reduce_scatter | solution.py:174
  (67 shorter events, 0.5 us)
Async XLA Ops:
  6.5 240.7 %copy-start = (bf16[1,512,512]{2,1,0:T(8,128)(2,1)S(1)}, bf16[1,512,512]{2,1,0:T(8,128)(2,1)}, u32[]{:S(2)}) copy-start(bf16[1,512,512]{2,1,0:T(8,128)(2,1)} %param.18) | copy-start | bytes 1572868
  6.5 129.9 %copy-start.7 = (bf16[512,512]{1,0:T(8,128)(2,1)S(1)}, bf16[512,512]{1,0:T(8,128)(2,1)}, u32[]{:S(2)}) copy-start(bf16[512,512]{1,0:T(8,128)(2,1)} %param.15) | copy-start | bytes 1572868
  6.5 77.5 %copy-start.10 = (bf16[512,64]{0,1:T(8,128)(2,1)S(1)}, bf16[512,64]{0,1:T(8,128)(2,1)}, u32[]{:S(2)}) copy-start(bf16[512,64]{0,1:T(8,128)(2,1)} %param.17) | copy-start | bytes 196612
  6.5 190.3 %all-gather.4.cloned.1.call-start = ((), (), s32[]{:S(2)}) async-start(), calls=%async_computation.1 | async-start | bytes 10485760 | tf_op jit(solution)/shard_map/all_gather | solution.py:59
  7.3 205.1 %all-gather.6.cloned.1.call-start = ((), (), s32[]{:S(2)}) async-start(), calls=%async_computation.2 | async-start | bytes 4718592 | tf_op jit(solution)/shard_map/all_gather | solution.py:64
  8.0 297.4 %all-gather.8.cloned.1.call-start = ((), (), s32[]{:S(2)}) async-start(), calls=%async_computation.3 | async-start | bytes 9437184 | tf_op jit(solution)/shard_map/all_gather | solution.py:173
  8.1 18.2 %collective-permute-start.2 = (bf16[512,512]{1,0:T(8,128)(2,1)}, bf16[512,512]{1,0:T(8,128)(2,1)S(1)}, u32[]{:S(2)}, u32[]{:S(2)}) collective-permute-start(bf16[512,512]{1,0:T(8,128)(2,1)} %param.15), channel_id=1, source_target_pairs={{0,4},{4,8},{8,12},{12,16},{16,20},{20,24},{24,28},{28,0},{1,5},{5... | collective-permute-start | bytes 1572872 | tf_op jit(solution)/shard_map/ppermute | solution.py:25
  11.1 378.5 %reduce-scatter.2.cloned.1.call-start = ((), (), s32[]{:S(2)}) async-start(), calls=%async_computation.4 | async-start | bytes 10485760 | tf_op jit(solution)/shard_map/reduce_scatter | solution.py:174
  26.3 15.8 %collective-permute-start.3 = (bf16[512,512]{1,0:T(8,128)(2,1)S(1)}, bf16[512,512]{1,0:T(8,128)(2,1)S(1)}, u32[]{:S(2)}, u32[]{:S(2)}) collective-permute-start(bf16[512,512]{1,0:T(8,128)(2,1)S(1)} %collective-permute-done.2), channel_id=1, source_target_pairs={{0,4},{4,8},{8,12},{12,16},{16,20},{20,24},{24,28},{28,0},{1,5},{5... | collective-permute-start | bytes 1572872 | tf_op jit(solution)/shard_map/ppermute | solution.py:25
  42.1 41.2 %collective-permute-start.4 = (bf16[512,512]{1,0:T(8,128)(2,1)S(1)}, bf16[512,512]{1,0:T(8,128)(2,1)S(1)}, u32[]{:S(2)}, u32[]{:S(2)}) collective-permute-start(bf16[512,512]{1,0:T(8,128)(2,1)S(1)} %collective-permute-done.3), channel_id=1, source_target_pairs={{0,4},{4,8},{8,12},{12,16},{16,20},{20,24},{24,28},{28,0},{1,5},{5... | collective-permute-start | bytes 1572872 | tf_op jit(solution)/shard_map/ppermute | solution.py:25
  83.3 0.8 copy-start.8
  83.3 52.3 %collective-permute-start.5 = (bf16[512,512]{1,0:T(8,128)(2,1)S(1)}, bf16[512,512]{1,0:T(8,128)(2,1)}, u32[]{:S(2)}, u32[]{:S(2)}) collective-permute-start(bf16[512,512]{1,0:T(8,128)(2,1)S(1)} %collective-permute-done.4), channel_id=1, source_target_pairs={{0,4},{4,8},{8,12},{12,16},{16,20},{20,24},{24,28},{28,0},{1,5},{5... | collective-permute-start | bytes 1572872 | tf_op jit(solution)/shard_map/ppermute | solution.py:25
  135.6 23.7 %collective-permute-start.6 = (bf16[512,512]{1,0:T(8,128)(2,1)}, bf16[512,512]{1,0:T(8,128)(2,1)}, u32[]{:S(2)}, u32[]{:S(2)}) collective-permute-start(bf16[512,512]{1,0:T(8,128)(2,1)} %collective-permute-done.5), channel_id=1, source_target_pairs={{0,4},{4,8},{8,12},{12,16},{16,20},{20,24},{24,28},{28,0},{1,5},{5... | collective-permute-start | bytes 1572872 | tf_op jit(solution)/shard_map/ppermute | solution.py:25
  135.7 25.3 %copy-start.9 = (bf16[512,512]{1,0:T(8,128)(2,1)S(1)}, bf16[512,512]{1,0:T(8,128)(2,1)}, u32[]{:S(2)}) copy-start(bf16[512,512]{1,0:T(8,128)(2,1)} %copy-done.8) | copy-start | bytes 1572868
  159.3 19.8 %collective-permute-start.7 = (bf16[512,512]{1,0:T(8,128)(2,1)}, bf16[512,512]{1,0:T(8,128)(2,1)S(1)}, u32[]{:S(2)}, u32[]{:S(2)}) collective-permute-start(bf16[512,512]{1,0:T(8,128)(2,1)} %collective-permute-done.6), channel_id=1, source_target_pairs={{0,4},{4,8},{8,12},{12,16},{16,20},{20,24},{24,28},{28,0},{1,5},{5... | collective-permute-start | bytes 1572872 | tf_op jit(solution)/shard_map/ppermute | solution.py:25
  179.1 12.0 %collective-permute-start.8 = (bf16[512,512]{1,0:T(8,128)(2,1)S(1)}, bf16[512,512]{1,0:T(8,128)(2,1)S(1)}, u32[]{:S(2)}, u32[]{:S(2)}) collective-permute-start(bf16[512,512]{1,0:T(8,128)(2,1)S(1)} %collective-permute-done.7), channel_id=1, source_target_pairs={{0,4},{4,8},{8,12},{12,16},{16,20},{20,24},{24,28},{28,0},{1,5},{5... | collective-permute-start | bytes 1572872 | tf_op jit(solution)/shard_map/ppermute | solution.py:25
  196.8 5.1 %copy-start.11 = (f32[4096]{0:T(1024)S(1)}, f32[4096]{0:T(1024)}, u32[]{:S(2)}) copy-start(f32[4096]{0:T(1024)} %param.13) | copy-start | bytes 49156
  212.4 10.9 %copy-start.2 = (bf16[1024,4096]{1,0:T(8,128)(2,1)S(1)}, bf16[1024,4096]{1,0:T(8,128)(2,1)}, u32[]{:S(2)}) copy-start(bf16[1024,4096]{1,0:T(8,128)(2,1)} %fusion.2) | copy-start | bytes 25165828
  221.6 4.3 %copy-start.4 = (bf16[1024,512]{1,0:T(8,128)(2,1)}, bf16[1024,512]{1,0:T(8,128)(2,1)S(1)}, u32[]{:S(2)}) copy-start(bf16[1024,512]{1,0:T(8,128)(2,1)S(1)} %convolution_convert_fusion.2) | copy-start | bytes 3145732
  221.6 4.4 %copy-start.12 = (f32[64]{0:T(128)S(1)}, f32[64]{0:T(128)}, u32[]{:S(2)}) copy-start(f32[64]{0:T(128)} %param.21) | copy-start | bytes 772
  221.7 24.2 %collective-permute-start = (bf16[15,512]{1,0:T(8,128)(2,1)S(1)}, bf16[15,512]{1,0:T(8,128)(2,1)S(1)}, u32[]{:S(2)}, u32[]{:S(2)}) collective-permute-start(bf16[15,512]{1,0:T(8,128)(2,1)S(1)} %slice.88), channel_id=1, source_target_pairs={{0,4},{4,8},{8,12},{12,16},{16,20},{20,24},{24,28},{1,5},{5,9},{9,... | collective-permute-start | bytes 46088 | tf_op jit(solution)/shard_map/ppermute | solution.py:34
  226.1 4.0 %copy-start.3 = (bf16[8,512,512]{2,1,0:T(8,128)(2,1)S(1)}, bf16[8,512,512]{2,1,0:T(8,128)(2,1)}, u32[]{:S(2)}) copy-start(bf16[8,512,512]{2,1,0:T(8,128)(2,1)} %gather_fusion) | copy-start | bytes 12582916
  228.8 21.6 %collective-permute-start.1 = (bf16[128,128]{0,1:T(8,128)(2,1)S(1)}, bf16[128,128]{0,1:T(8,128)(2,1)S(1)}, u32[]{:S(2)}, u32[]{:S(2)}) collective-permute-start(bf16[128,128]{0,1:T(8,128)(2,1)S(1)} %pad_maximum_fusion.3), channel_id=1, source_target_pairs={{0,4},{4,8},{8,12},{12,16},{16,20},{20,24},{24,28},{1,5},{5,9},{9,... | collective-permute-start | bytes 98312 | tf_op jit(solution)/shard_map/ppermute | solution.py:34
  242.9 2.5 copy-start.14
  244.8 1.2 copy-start.5
  246.9 0.7 copy-start.13
  249.0 1.4 copy-start.6
  319.9 69.7 %copy-start.1 = (bf16[1,512,512]{2,1,0:T(8,128)(2,1)S(1)}, bf16[1,512,512]{2,1,0:T(8,128)(2,1)}, u32[]{:S(2)}) copy-start(bf16[1,512,512]{2,1,0:T(8,128)(2,1)} %param.18) | copy-start | bytes 1572868
Sparse Core Ops, SparseCore 0:
  8.9 60.9 all-gather.3
  72.0 97.2 all-gather.5
  171.3 134.0 all-gather.7
  320.0 69.5 reduce-scatter.1
